TPU v7x, 256 devices: a whole 4x4x8 slice. The times are simulated.
256 devices in a mesh: sp: 32 (over z, y), tp: 8 (over x, core).
Axes of the slice: x: 4, y: 4, z: 8, core: 2. Of those that a mesh axis runs over, the one named last changes fastest.
Arguments:
- tokens: bfloat16 [24576, 4096], P('sp', 'tp'), may hold values from -6 to 6
- in_proj: bfloat16 [3, 4096, 1024], P(None, 'tp', 'sp'), may hold values from -0.09375 to 0.09375
- group_mix: bfloat16 [3, 4, 256, 256], replicated, may hold values from -0.375 to 0.375
- pool_gain: float32 [3, 1024], replicated, may hold values from 0.1 to 1.9
- out_proj: bfloat16 [3, 1024, 4096], P(None, 'sp', 'tp'), may hold values from -0.1875 to 0.1875
- norm_gain: float32 [3, 4096], P(None, 'tp'), may hold values from 0.25 to 3
- norm_bias: float32 [3, 4096], P(None, 'tp'), may hold values from -1.5 to 1.5
Outputs:
- stream_out: bfloat16 [24576, 4096], P('sp', 'tp')
All inputs are finite; a program needn't handle non-finite values.
Results may differ from a plain program's by a relative error of at most 0.017.
Values may be sent and summed in bfloat16 or wider, within the bound.
No kernel may reach another device: no remote copies, remote signals or barrier semaphores. Data moves between devices by JAX's collectives and lax.ppermute only.
A program may use at most 128 MiB of HBM per device.

v0:
```python
import jax
import jax.numpy as jnp
from jax import lax
from jax.sharding import Mesh
from jax.sharding import PartitionSpec as P

SP = ("sp_0", "sp_1")


pool_windows = (2, 4, 8, 16)
norm_eps = 1e-05


def gather_axes(array, axes, dim):
    for axis in reversed(axes):
        array = lax.all_gather(array, axis, axis=dim, tiled=True)
    return array


def cut_along(array, dim, devices):
    before, after = (array.shape[:dim], array.shape[dim + 1 :])
    return jnp.moveaxis(array.reshape(*before, devices, -1, *after), dim, 0)


def summed_on_arrival(array, axis, dim):
    blocks = cut_along(array, dim, lax.axis_size(axis))
    arrived = lax.all_to_all(blocks, axis, split_axis=0, concat_axis=0, tiled=True)
    return arrived.astype(jnp.float32).sum(axis=0)


def padded(array, sides, width):
    for axis, dim in sides:
        devices, length = (lax.axis_size(axis), array.shape[dim])
        up = [(i, (i + 1) % devices) for i in range(devices - 1)]
        down = [(j, i) for i, j in up]
        last = lax.slice_in_dim(array, length - width, length, axis=dim)
        leading = lax.slice_in_dim(array, 0, width, axis=dim)
        before = lax.ppermute(last, axis, up)
        after = lax.ppermute(leading, axis, down)
        array = jnp.concatenate([before, array, after], axis=dim)
    return array


def sent_to_all(array, axis):
    devices = lax.axis_size(axis)
    return lax.all_to_all(
        jnp.broadcast_to(array[None], (devices, *array.shape)), axis, 0, 0, tiled=True
    )


def joined_along(blocks, dim):
    lengths = list(blocks.shape[1:])
    lengths[dim] *= blocks.shape[0]
    return jnp.moveaxis(blocks, 0, dim).reshape(lengths)


def gather_directly(array, axis, dim):
    blocks = sent_to_all(array, axis)
    return joined_along(blocks, dim)


def taken_together(array, axis):
    return sent_to_all(array, axis).sum(axis=0)


def packed_total(arrays, axis):
    ends = [0]
    for a in arrays:
        ends.append(ends[-1] + a.size)
    running = taken_together(jnp.concatenate([a.ravel() for a in arrays]), axis)
    return tuple((running[b:e].reshape(a.shape) for a, b, e in zip(arrays, ends, ends[1:])))


def on_device(tokens, in_proj, group_mix, pool_gain, out_proj, norm_gain, norm_bias):
    rows_dev = tokens.shape[0]
    feat_dev = tokens.shape[1]
    layer_count = in_proj.shape[0]
    pool_width = in_proj.shape[2] * lax.axis_size(SP)
    chan_share = pool_width // lax.axis_size("tp")
    group_width = group_mix.shape[2]
    model_width = feat_dev * lax.axis_size("tp")
    residual_scale = (2.0 * layer_count) ** 0.25
    fringe_width = max(pool_windows) // 2
    seq_length = rows_dev * lax.axis_size(SP)
    positions = lax.axis_index(SP) * rows_dev + jnp.arange(rows_dev)
    chan_groups = (lax.axis_index("tp") * chan_share + jnp.arange(chan_share)) // group_width
    in_all, out_all = (gather_axes(in_proj, SP, 2), gather_axes(out_proj, SP, 1))
    stream = tokens
    for layer_idx in range(layer_count):
        in_block = in_all[layer_idx]
        out_block = out_all[layer_idx]
        projected = summed_on_arrival(
            lax.dot_general(
                in_block, stream, (((0,), (1,)), ((), ())), preferred_element_type=jnp.float32
            ).astype(jnp.bfloat16),
            "tp",
            0,
        ).astype(jnp.bfloat16)
        extended = padded(projected, ((SP, 1),), fringe_width)
        ext_float = extended.astype(jnp.float32)
        pooled = jnp.zeros((chan_share, rows_dev), jnp.float32)
        for group_idx in range(4):
            own_rows = (chan_groups == group_idx)[:, None]
            span_len = pool_windows[group_idx]
            before = span_len // 2
            after = span_len - before
            window_total = jnp.zeros((ext_float.shape[0], rows_dev), jnp.float32)
            for offset in range(-before, after):
                window_total = (
                    window_total
                    + ext_float[:, fringe_width + offset : fringe_width + offset + rows_dev]
                )
            low_edge = jnp.clip(positions - before, 0, seq_length)
            high_edge = jnp.clip(positions + after, 0, seq_length)
            pooled = jnp.where(
                own_rows, window_total / (high_edge - low_edge).astype(jnp.float32)[None, :], pooled
            )
        differ = (pooled - projected.astype(jnp.float32)).astype(jnp.bfloat16)
        all_differ = gather_directly(differ, "tp", 0)
        grouped = all_differ.reshape(4, group_width, rows_dev)
        mixed_all = jnp.einsum(
            "gcd,gct->gdt", group_mix[layer_idx], grouped, preferred_element_type=jnp.float32
        ).reshape(pool_width, rows_dev)
        mixed_all = (mixed_all * pool_gain[layer_idx][:, None]).astype(jnp.bfloat16)
        branch = lax.dot_general(
            mixed_all, out_block, (((0,), (0,)), ((), ())), preferred_element_type=jnp.float32
        )
        resid = residual_scale * stream.astype(jnp.float32) + branch
        row_sums, squares = packed_total(
            (jnp.sum(resid, axis=1), jnp.sum(resid * resid, axis=1)), "tp"
        )
        row_mean = row_sums / model_width
        row_var = squares / model_width - row_mean * row_mean
        normed = (resid - row_mean[:, None]) * lax.rsqrt(row_var[:, None] + norm_eps)
        stream = (normed * norm_gain[layer_idx][None, :] + norm_bias[layer_idx][None, :]).astype(
            jnp.bfloat16
        )
    return stream


def solution(mesh):
    split = Mesh(mesh.devices.reshape(8, 4, mesh.shape["tp"]), ("sp_0", "sp_1", "tp"))
    in_specs = (
        P(SP, "tp"),
        P(None, "tp", SP),
        P(),
        P(),
        P(None, SP, "tp"),
        P(None, "tp"),
        P(None, "tp"),
    )
    out_specs = P(SP, "tp")
    return jax.shard_map(
        on_device, mesh=split, in_specs=in_specs, out_specs=out_specs, check_vma=False
    )
```

profile of v0, /device:TPU:128, one launch (start us, length us, event | category | flops | bytes accessed | tf_op | source)
XLA Modules:
  0.0 321.4 jit_solution(1923683457139125775)
XLA Ops:
  6.5 14.9 %all_gather.12 = bf16[3,512,128]{1,2,0:T(8,128)(2,1)} all-gather(bf16[3,512,32]{1,2,0:T(8,128)(2,1)} %param.8), channel_id=1, replica_groups=mesh['sp_0'=8,'sp_1'=4,'tp'=8] {'sp_1'}, dimensions={2}, use_global_device_ids=true | all-gather | bytes 491520 | tf_op jit(solution)/shard_map/all_gather | solution.py:16
  21.5 13.5 %all_gather.14 = bf16[3,128,512]{2,1,0:T(8,128)(2,1)} all-gather(bf16[3,32,512]{2,1,0:T(8,128)(2,1)} %param.11), channel_id=1, replica_groups=mesh['sp_0'=8,'sp_1'=4,'tp'=8] {'sp_1'}, dimensions={1}, use_global_device_ids=true | all-gather | bytes 491520 | tf_op jit(solution)/shard_map/all_gather | solution.py:16
  35.0 28.9 %all-gather.3.cloned.1.call-done = bf16[3,512,1024]{1,2,0:T(8,128)(2,1)} async-done(((bf16[3,512,128]{1,2,0:T(8,128)(2,1)}), bf16[3,512,1024]{1,2,0:T(8,128)(2,1)}) %all-gather.3.cloned.1.call-update) | async-done | bytes 3145744 | tf_op jit(solution)/shard_map/all_gather | solution.py:16
  64.0 3.4 %convolution_convert_fusion.2 = bf16[1024,768]{1,0:T(8,128)(2,1)} fusion(bf16[768,512]{1,0:T(8,128)(2,1)S(1)} %copy-done.1, bf16[3,512,1024]{1,2,0:T(8,128)(2,1)} %all-gather.3.cloned.1.call-done), kind=kOutput, calls=%fused_computation.5 | convolution fusion | flops 806092800 | bytes 3407872 | tf_op jit(solution)/shard_map/dot_general | solution.py:93
  67.3 4.3 %all-to-all-start = ((bf16[8,128,768]{2,1,0:T(8,128)(2,1)}), bf16[8,128,768]{2,1,0:T(8,128)(2,1)S(1)}, u32[]{:S(2)}, u32[]{:S(2)}) async-start(bf16[8,128,768]{2,1,0:T(8,128)(2,1)} %bitcast.1), calls=%async_computation | async-start | bytes 3145728 | tf_op jit(solution)/shard_map/all_to_all | solution.py:27
  71.7 21.5 %all-to-all-done = bf16[8,128,768]{2,1,0:T(8,128)(2,1)S(1)} async-done(((bf16[8,128,768]{2,1,0:T(8,128)(2,1)}), bf16[8,128,768]{2,1,0:T(8,128)(2,1)S(1)}, u32[]{:S(2)}, u32[]{:S(2)}) %all-to-all-start) | async-done | bytes 1572896 | tf_op jit(solution)/shard_map/all_to_all | solution.py:27
  93.5 3.4 %collective-permute-start = (bf16[128,8]{1,0:T(8,128)(2,1)S(1)}, bf16[128,8]{1,0:T(8,128)(2,1)S(1)}, u32[]{:S(2)}, u32[]{:S(2)}) collective-permute-start(bf16[128,8]{1,0:T(8,128)(2,1)S(1)} %get-tuple-element.18), channel_id=1, source_target_pairs={{0,8},{8,16},{16,24},{24,32},{32,40},{40,48},{48,56},{56,64},{64,7... | collective-permute-start | bytes 6152 | tf_op jit(solution)/shard_map/ppermute | solution.py:38
  96.9 5.8 %collective-permute-start.1 = (bf16[128,8]{1,0:T(8,128)(2,1)S(1)}, bf16[128,8]{1,0:T(8,128)(2,1)S(1)}, u32[]{:S(2)}, u32[]{:S(2)}) collective-permute-start(bf16[128,8]{1,0:T(8,128)(2,1)S(1)} %get-tuple-element.19), channel_id=1, source_target_pairs={{8,0},{16,8},{24,16},{32,24},{40,32},{48,40},{56,48},{64,56},{72,6... | collective-permute-start | bytes 6152 | tf_op jit(solution)/shard_map/ppermute | solution.py:39
  107.9 3.7 %all-to-all-start.1 = ((bf16[8,128,768]{2,1,0:T(8,128)(2,1)}), bf16[8,128,768]{2,1,0:T(8,128)(2,1)S(1)}, u32[]{:S(2)}, u32[]{:S(2)}) async-start(bf16[8,128,768]{2,1,0:T(8,128)(2,1)} %broadcast_in_dim.117), calls=%async_computation.1 | async-start | bytes 3145728 | tf_op jit(solution)/shard_map/all_to_all | solution.py:46
  112.9 20.2 %all-to-all-done.1 = bf16[8,128,768]{2,1,0:T(8,128)(2,1)S(1)} async-done(((bf16[8,128,768]{2,1,0:T(8,128)(2,1)}), bf16[8,128,768]{2,1,0:T(8,128)(2,1)S(1)}, u32[]{:S(2)}, u32[]{:S(2)}) %all-to-all-start.1) | async-done | bytes 1572896 | tf_op jit(solution)/shard_map/all_to_all | solution.py:46
  133.1 1.7 multiply_convert_fusion.2
  134.8 3.7 %fusion.55 = (f32[768]{0:T(1024)S(1)}, f32[768]{0:T(1024)S(1)}, f32[768,512]{0,1:T(8,128)}) fusion(bf16[1024,768]{1,0:T(8,128)(2,1)S(1)} %bitcast.80, bf16[3,1024,512]{2,1,0:T(8,128)(2,1)} %all-gather.5.cloned.1.call-done, bf16[768,512]{0,1:T(8,128)(2,1)} %copy.59), kind=kOutput, calls=%fused_computation.127 | convolution fusion | flops 807664128 | bytes 4986880 | tf_op jit(solution)/shard_map/dot_general | solution.py:125
  139.2 3.3 %all-to-all-start.2 = ((f32[8,1,1536]{2,1,0:T(1,128)}), f32[8,1,1536]{2,1,0:T(1,128)S(1)}, u32[]{:S(2)}, u32[]{:S(2)}) async-start(f32[8,1,1536]{2,1,0:T(1,128)} %broadcast_in_dim.118), calls=%async_computation.2 | async-start | bytes 98304 | tf_op jit(solution)/shard_map/all_to_all | solution.py:46
  142.6 5.4 %all-to-all-done.2 = f32[8,1,1536]{2,1,0:T(1,128)S(1)} async-done(((f32[8,1,1536]{2,1,0:T(1,128)}), f32[8,1,1536]{2,1,0:T(1,128)S(1)}, u32[]{:S(2)}, u32[]{:S(2)}) %all-to-all-start.2) | async-done | bytes 49184 | tf_op jit(solution)/shard_map/all_to_all | solution.py:46
  148.1 3.0 fusion
  151.3 24.0 %all_to_all.48 = bf16[8,128,768]{1,2,0:T(8,128)(2,1)S(1)} all-to-all(bf16[8,128,768]{1,2,0:T(8,128)(2,1)S(1)} %bitcast.77), channel_id=1, replica_groups=mesh['sp_0'=8,'sp_1'=4,'tp'=8] {'tp'}, dimensions={0} | all-to-all | bytes 3145728 | tf_op jit(solution)/shard_map/all_to_all | solution.py:27
  175.9 7.7 %collective-permute-start.3 = (bf16[128,8]{1,0:T(8,128)(2,1)S(1)}, bf16[128,8]{1,0:T(8,128)(2,1)S(1)}, u32[]{:S(2)}, u32[]{:S(2)}) collective-permute-start(bf16[128,8]{1,0:T(8,128)(2,1)S(1)} %copy.65), channel_id=1, source_target_pairs={{8,0},{16,8},{24,16},{32,24},{40,32},{48,40},{56,48},{64,56},{72,6... | collective-permute-start | bytes 6152 | tf_op jit(solution)/shard_map/ppermute | solution.py:39
  183.6 1.9 collective-permute-start.2
  185.7 7.0 %collective-permute-done.2 = bf16[128,8]{1,0:T(8,128)(2,1)S(1)} collective-permute-done((bf16[128,8]{1,0:T(8,128)(2,1)S(1)}, bf16[128,8]{1,0:T(8,128)(2,1)S(1)}, u32[]{:S(2)}, u32[]{:S(2)}) %collective-permute-start.2) | collective-permute-done | bytes 2080 | tf_op jit(solution)/shard_map/ppermute | solution.py:38
  195.9 3.9 %all-to-all-start.4 = ((bf16[8,128,768]{2,1,0:T(8,128)(2,1)}), bf16[8,128,768]{2,1,0:T(8,128)(2,1)S(1)}, u32[]{:S(2)}, u32[]{:S(2)}) async-start(bf16[8,128,768]{2,1,0:T(8,128)(2,1)} %broadcast_in_dim.119), calls=%async_computation.4 | async-start | bytes 3145728 | tf_op jit(solution)/shard_map/all_to_all | solution.py:46
  199.8 21.3 %all-to-all-done.4 = bf16[8,128,768]{2,1,0:T(8,128)(2,1)S(1)} async-done(((bf16[8,128,768]{2,1,0:T(8,128)(2,1)}), bf16[8,128,768]{2,1,0:T(8,128)(2,1)S(1)}, u32[]{:S(2)}, u32[]{:S(2)}) %all-to-all-start.4) | async-done | bytes 1572896 | tf_op jit(solution)/shard_map/all_to_all | solution.py:46
  222.5 3.7 %fusion.54 = (f32[768]{0:T(1024)S(1)}, f32[768]{0:T(1024)S(1)}, f32[768,512]{0,1:T(8,128)}) fusion(bf16[1024,768]{1,0:T(8,128)(2,1)S(1)} %bitcast.81, bf16[3,1024,512]{2,1,0:T(8,128)(2,1)} %all-gather.5.cloned.1.call-done, f32[512]{0:T(512)S(1)} %bitcast.91, f32[512]{0:T(512)S(1)} %bitcast.89, f32[768]{0:T(1024)S(1)} %get-tuple-element.31, ...), kind=kOutput, calls=%fused_computation.126 | convolution fusion | flops 809630208 | bytes 5783552 | tf_op jit(solution)/shard_map/dot_general | solution.py:125
  226.2 7.9 %all_to_all.49 = f32[8,1,1536]{2,1,0:T(1,128)S(1)} all-to-all(f32[8,1,1536]{2,1,0:T(1,128)S(1)} %broadcast_in_dim.120), channel_id=1, replica_groups=mesh['sp_0'=8,'sp_1'=4,'tp'=8] {'tp'}, dimensions={0} | all-to-all | bytes 98304 | tf_op jit(solution)/shard_map/all_to_all | solution.py:46
  234.2 3.0 fusion.1
  237.4 24.0 %all_to_all.50 = bf16[8,128,768]{1,2,0:T(8,128)(2,1)S(1)} all-to-all(bf16[8,128,768]{1,2,0:T(8,128)(2,1)S(1)} %bitcast.78), channel_id=1, replica_groups=mesh['sp_0'=8,'sp_1'=4,'tp'=8] {'tp'}, dimensions={0} | all-to-all | bytes 3145728 | tf_op jit(solution)/shard_map/all_to_all | solution.py:27
  262.0 1.9 collective-permute-start.5
  263.9 3.9 %collective-permute-start.4 = (bf16[128,8]{1,0:T(8,128)(2,1)S(1)}, bf16[128,8]{1,0:T(8,128)(2,1)S(1)}, u32[]{:S(2)}, u32[]{:S(2)}) collective-permute-start(bf16[128,8]{1,0:T(8,128)(2,1)S(1)} %copy.72), channel_id=1, source_target_pairs={{0,8},{8,16},{16,24},{24,32},{32,40},{40,48},{48,56},{56,64},{64,7... | collective-permute-start | bytes 6152 | tf_op jit(solution)/shard_map/ppermute | solution.py:38
  268.0 5.0 %collective-permute-done.4 = bf16[128,8]{1,0:T(8,128)(2,1)S(1)} collective-permute-done((bf16[128,8]{1,0:T(8,128)(2,1)S(1)}, bf16[128,8]{1,0:T(8,128)(2,1)S(1)}, u32[]{:S(2)}, u32[]{:S(2)}) %collective-permute-start.4) | collective-permute-done | bytes 2080 | tf_op jit(solution)/shard_map/ppermute | solution.py:38
  276.1 3.6 %all-to-all-start.7 = ((bf16[8,128,768]{2,1,0:T(8,128)(2,1)}), bf16[8,128,768]{2,1,0:T(8,128)(2,1)S(1)}, u32[]{:S(2)}, u32[]{:S(2)}) async-start(bf16[8,128,768]{2,1,0:T(8,128)(2,1)} %broadcast_in_dim.121), calls=%async_computation.7 | async-start | bytes 3145728 | tf_op jit(solution)/shard_map/all_to_all | solution.py:46
  279.7 21.5 %all-to-all-done.7 = bf16[8,128,768]{2,1,0:T(8,128)(2,1)S(1)} async-done(((bf16[8,128,768]{2,1,0:T(8,128)(2,1)}), bf16[8,128,768]{2,1,0:T(8,128)(2,1)S(1)}, u32[]{:S(2)}, u32[]{:S(2)}) %all-to-all-start.7) | async-done | bytes 1572896 | tf_op jit(solution)/shard_map/all_to_all | solution.py:46
  302.6 2.6 fusion.53
  305.2 7.9 %all_to_all.51 = f32[8,1,1536]{2,1,0:T(1,128)S(1)} all-to-all(f32[8,1,1536]{2,1,0:T(1,128)S(1)} %broadcast_in_dim.122), channel_id=1, replica_groups=mesh['sp_0'=8,'sp_1'=4,'tp'=8] {'tp'}, dimensions={0} | all-to-all | bytes 98304 | tf_op jit(solution)/shard_map/all_to_all | solution.py:46
  (73 shorter events, 20.2 us)
Async XLA Ops:
  6.5 57.4 %copy-start.1 = (bf16[768,512]{1,0:T(8,128)(2,1)S(1)}, bf16[768,512]{1,0:T(8,128)(2,1)}, u32[]{:S(2)}) copy-start(bf16[768,512]{1,0:T(8,128)(2,1)} %param.7) | copy-start | bytes 2359300
  6.5 57.4 %all-gather.3.cloned.1.call-start = ((), (), s32[]{:S(2)}) async-start(), calls=%async_computation.9 | async-start | bytes 3538944 | tf_op jit(solution)/shard_map/all_gather | solution.py:16
  21.5 113.3 %all-gather.5.cloned.1.call-start = ((), (), s32[]{:S(2)}) async-start(), calls=%async_computation.10 | async-start | bytes 3538944 | tf_op jit(solution)/shard_map/all_gather | solution.py:16
  67.3 25.8 %all-to-all-start = ((bf16[8,128,768]{2,1,0:T(8,128)(2,1)}), bf16[8,128,768]{2,1,0:T(8,128)(2,1)S(1)}, u32[]{:S(2)}, u32[]{:S(2)}) async-start(bf16[8,128,768]{2,1,0:T(8,128)(2,1)} %bitcast.1), calls=%async_computation | async-start | bytes 3145728 | tf_op jit(solution)/shard_map/all_to_all | solution.py:27
  93.5 9.9 %collective-permute-start = (bf16[128,8]{1,0:T(8,128)(2,1)S(1)}, bf16[128,8]{1,0:T(8,128)(2,1)S(1)}, u32[]{:S(2)}, u32[]{:S(2)}) collective-permute-start(bf16[128,8]{1,0:T(8,128)(2,1)S(1)} %get-tuple-element.18), channel_id=1, source_target_pairs={{0,8},{8,16},{16,24},{24,32},{32,40},{40,48},{48,56},{56,64},{64,7... | collective-permute-start | bytes 6152 | tf_op jit(solution)/shard_map/ppermute | solution.py:38
  96.9 8.0 %collective-permute-start.1 = (bf16[128,8]{1,0:T(8,128)(2,1)S(1)}, bf16[128,8]{1,0:T(8,128)(2,1)S(1)}, u32[]{:S(2)}, u32[]{:S(2)}) collective-permute-start(bf16[128,8]{1,0:T(8,128)(2,1)S(1)} %get-tuple-element.19), channel_id=1, source_target_pairs={{8,0},{16,8},{24,16},{32,24},{40,32},{48,40},{56,48},{64,56},{72,6... | collective-permute-start | bytes 6152 | tf_op jit(solution)/shard_map/ppermute | solution.py:39
  107.9 4.9 %copy-start.2 = (f32[3,1024]{1,0:T(4,128)S(1)}, f32[3,1024]{1,0:T(4,128)}, u32[]{:S(2)}) copy-start(f32[3,1024]{1,0:T(4,128)} %param.10) | copy-start | bytes 36868
  107.9 25.2 %all-to-all-start.1 = ((bf16[8,128,768]{2,1,0:T(8,128)(2,1)}), bf16[8,128,768]{2,1,0:T(8,128)(2,1)S(1)}, u32[]{:S(2)}, u32[]{:S(2)}) async-start(bf16[8,128,768]{2,1,0:T(8,128)(2,1)} %broadcast_in_dim.117), calls=%async_computation.1 | async-start | bytes 3145728 | tf_op jit(solution)/shard_map/all_to_all | solution.py:46
  111.6 1.2 copy-start.3
  134.8 7.7 %copy-start.4 = (f32[3,512]{1,0:T(4,128)S(1)}, f32[3,512]{1,0:T(4,128)}, u32[]{:S(2)}) copy-start(f32[3,512]{1,0:T(4,128)} %param.13) | copy-start | bytes 18436
  139.2 8.8 %all-to-all-start.2 = ((f32[8,1,1536]{2,1,0:T(1,128)}), f32[8,1,1536]{2,1,0:T(1,128)S(1)}, u32[]{:S(2)}, u32[]{:S(2)}) async-start(f32[8,1,1536]{2,1,0:T(1,128)} %broadcast_in_dim.118), calls=%async_computation.2 | async-start | bytes 98304 | tf_op jit(solution)/shard_map/all_to_all | solution.py:46
  175.9 9.8 %collective-permute-start.3 = (bf16[128,8]{1,0:T(8,128)(2,1)S(1)}, bf16[128,8]{1,0:T(8,128)(2,1)S(1)}, u32[]{:S(2)}, u32[]{:S(2)}) collective-permute-start(bf16[128,8]{1,0:T(8,128)(2,1)S(1)} %copy.65), channel_id=1, source_target_pairs={{8,0},{16,8},{24,16},{32,24},{40,32},{48,40},{56,48},{64,56},{72,6... | collective-permute-start | bytes 6152 | tf_op jit(solution)/shard_map/ppermute | solution.py:39
  183.6 9.1 %collective-permute-start.2 = (bf16[128,8]{1,0:T(8,128)(2,1)S(1)}, bf16[128,8]{1,0:T(8,128)(2,1)S(1)}, u32[]{:S(2)}, u32[]{:S(2)}) collective-permute-start(bf16[128,8]{1,0:T(8,128)(2,1)S(1)} %copy.64), channel_id=1, source_target_pairs={{0,8},{8,16},{16,24},{24,32},{32,40},{40,48},{48,56},{56,64},{64,7... | collective-permute-start | bytes 6152 | tf_op jit(solution)/shard_map/ppermute | solution.py:38
  195.9 25.2 %copy-start = (bf16[3,4,256,256]{3,2,1,0:T(8,128)(2,1)S(1)}, bf16[3,4,256,256]{3,2,1,0:T(8,128)(2,1)}, u32[]{:S(2)}) copy-start(bf16[3,4,256,256]{3,2,1,0:T(8,128)(2,1)} %param.9) | copy-start | bytes 4718596
  195.9 25.2 %all-to-all-start.4 = ((bf16[8,128,768]{2,1,0:T(8,128)(2,1)}), bf16[8,128,768]{2,1,0:T(8,128)(2,1)S(1)}, u32[]{:S(2)}, u32[]{:S(2)}) async-start(bf16[8,128,768]{2,1,0:T(8,128)(2,1)} %broadcast_in_dim.119), calls=%async_computation.4 | async-start | bytes 3145728 | tf_op jit(solution)/shard_map/all_to_all | solution.py:46
  221.1 1.4 copy-start.6
  262.0 6.0 %collective-permute-start.5 = (bf16[128,8]{1,0:T(8,128)(2,1)S(1)}, bf16[128,8]{1,0:T(8,128)(2,1)S(1)}, u32[]{:S(2)}, u32[]{:S(2)}) collective-permute-start(bf16[128,8]{1,0:T(8,128)(2,1)S(1)} %copy.73), channel_id=1, source_target_pairs={{8,0},{16,8},{24,16},{32,24},{40,32},{48,40},{56,48},{64,56},{72,6... | collective-permute-start | bytes 6152 | tf_op jit(solution)/shard_map/ppermute | solution.py:39
  263.9 9.1 %collective-permute-start.4 = (bf16[128,8]{1,0:T(8,128)(2,1)S(1)}, bf16[128,8]{1,0:T(8,128)(2,1)S(1)}, u32[]{:S(2)}, u32[]{:S(2)}) collective-permute-start(bf16[128,8]{1,0:T(8,128)(2,1)S(1)} %copy.72), channel_id=1, source_target_pairs={{0,8},{8,16},{16,24},{24,32},{32,40},{40,48},{48,56},{56,64},{64,7... | collective-permute-start | bytes 6152 | tf_op jit(solution)/shard_map/ppermute | solution.py:38
  276.1 25.1 %all-to-all-start.7 = ((bf16[8,128,768]{2,1,0:T(8,128)(2,1)}), bf16[8,128,768]{2,1,0:T(8,128)(2,1)S(1)}, u32[]{:S(2)}, u32[]{:S(2)}) async-start(bf16[8,128,768]{2,1,0:T(8,128)(2,1)} %broadcast_in_dim.121), calls=%async_computation.7 | async-start | bytes 3145728 | tf_op jit(solution)/shard_map/all_to_all | solution.py:46
  301.2 1.4 copy-start.5
Sparse Core Ops, SparseCore 0:
  21.6 42.3 all-gather.2
  65.8 44.2 all-gather.4
where the time goes:
time: 323 us; the launch traced here: 321 us
  waiting for transfers between devices  133 us (41%)
  blocking collectives  92.2 us (29%)
  starting transfers between devices  43.4 us (13%)
  matrix products  22.2 us (7%)
  between operations  13.8 us (4%)
  local copies, waits for them, and re-layouts  9.94 us (3%)
  other arithmetic  6.67 us (2%)
    all_to_all x4, waiting for transfers between devices, sent_to_all(): lax.all_to_all(jnp.broadcast_to(array[None], (devices, *array.shape)), ax...  68.4 us
    all_to_all x2, blocking collectives, summed_on_arrival(): lax.all_to_all(blocks, axis, split_axis=0, concat_axis=0, tiled=True)  48 us
    all_gather x2, waiting for transfers between devices, gather_axes(): array = lax.all_gather(array, axis, axis=dim, tiled=True)  29 us
    all_gather x2, blocking collectives, gather_axes(): array = lax.all_gather(array, axis, axis=dim, tiled=True)  28.4 us
    all_to_all x1, waiting for transfers between devices, summed_on_arrival(): lax.all_to_all(blocks, axis, split_axis=0, concat_axis=0, tiled=True)  21.5 us
    all_to_all x2, blocking collectives, sent_to_all(): lax.all_to_all(jnp.broadcast_to(array[None], (devices, *array.shape)), ax...  15.8 us
    ppermute x3, starting transfers between devices, padded(): after = lax.ppermute(leading, axis, down)  15.4 us
    all_to_all x4, starting transfers between devices, sent_to_all(): lax.all_to_all(jnp.broadcast_to(array[None], (devices, *array.shape)), ax...  14.5 us
  transfers between devices with their start and end apart: 13, of which 10 were waited for; matrix products, arithmetic and copies ran while one was open for 3% of the time, Pallas kernels for 0%

commit v1 on v0

v1 whole, which is shorter than its diff:
```python
import functools

import jax
import jax.numpy as jnp
from jax import lax
from jax.experimental import pallas as pl
from jax.experimental.pallas import tpu as pltpu
from jax.sharding import Mesh
from jax.sharding import PartitionSpec as P

SP = ("z", "y")
norm_eps = 1e-05
REACH = 8
STAT = 16
F32, BF16 = jnp.float32, jnp.bfloat16


def nbytes(shapes):
    return sum(s.size * s.dtype.itemsize for s in shapes)


def kernel_call(body, out_shape, scratch=(), flops=0, in_specs=None, name=None, out_specs=None):
    def call(*args):
        specs = in_specs
        if specs is None:
            specs = [pl.BlockSpec(memory_space=pltpu.SMEM)]
            specs += [pl.BlockSpec(memory_space=pltpu.VMEM) for _ in args[1:]]
        outs = out_shape if isinstance(out_shape, (list, tuple)) else [out_shape]
        kw = {} if out_specs is None else {"out_specs": out_specs}
        return pl.pallas_call(
            body,
            out_shape=out_shape,
            in_specs=specs,
            scratch_shapes=list(scratch),
            cost_estimate=pl.CostEstimate(
                flops=flops, bytes_accessed=nbytes(args) + nbytes(outs), transcendentals=0
            ),
            name=name,
            **kw,
        )(*args)

    return call


def dot(a, b):
    return lax.dot_general(a, b, (((1,), (0,)), ((), ())), preferred_element_type=F32)


def dot_t(a, b):
    return lax.dot_general(a, b, (((1,), (1,)), ((), ())), preferred_element_type=F32)


def parts(v):
    hi = v.astype(BF16).astype(F32)
    mid = (v - hi).astype(BF16).astype(F32)
    low = (v - hi - mid).astype(BF16).astype(F32)
    return hi, mid, low


def project_body(sc, own, oth, w_own, w_oth, *outs):
    n = len(outs)
    width = outs[0].shape[1]
    for k in range(n):
        rows = pl.ds(((sc[0] + k) % n) * width, width)
        acc = dot_t(own[...], w_own[rows, :]) + dot_t(oth[...], w_oth[rows, :])
        outs[k][...] = acc.astype(BF16)


def pooled_mix(sc, proj, group_map, gain, out, seq_length):
    rows_in, rows_out = proj.shape[0], out.shape[0]
    half = lax.shift_left(jnp.int32(1), sc[0])
    base = sc[1]
    row = lax.broadcasted_iota(jnp.int32, (rows_out, rows_in), 0)
    col = lax.broadcasted_iota(jnp.int32, (rows_out, rows_in), 1) - REACH
    token = base + col
    inside = (col >= row - half) & (col < row + half) & (token >= 0) & (token < seq_length)
    band = jnp.where(inside, 1.0, 0.0).astype(BF16)
    at = base + lax.broadcasted_iota(jnp.int32, (rows_out, 1), 0)
    count = jnp.minimum(at + half, seq_length) - jnp.maximum(at - half, 0)
    count = jnp.maximum(count, 1).astype(F32)
    centre = proj.astype(F32)[REACH : REACH + rows_out]
    differ = (dot(band, proj) / count - centre).astype(BF16)
    out[...] = (dot(differ, group_map[...]) * gain[...]).astype(BF16)


def mix_first_body(sc, *refs, seq_length):
    *partials, group_map, gain, out = refs
    total = partials[0][...].astype(F32)
    for p in partials[1:]:
        total = total + p[...].astype(F32)
    pooled_mix(sc, total.astype(BF16), group_map, gain, out, seq_length)


def combine_stats(means, seconds, width):
    n = len(means)
    mean = means[0]
    for m in means[1:]:
        mean = mean + m
    mean = mean / n
    second = seconds[0] + width * jnp.square(means[0] - mean)
    for m, s in zip(means[1:], seconds[1:]):
        second = second + s + width * jnp.square(m - mean)
    return mean, lax.rsqrt(second / (n * width) + norm_eps)


def mix_body(sc, *refs, seq_length, width):
    *partials, group_map, gain, out, row_out = refs
    n = len(partials)
    rows = partials[0].shape[0] - 2 * STAT
    means, seconds, gw = [], [], []
    total, bw = None, None
    for p in partials:
        stat = jnp.concatenate(
            [p[rows : rows + STAT, :].astype(F32), p[rows + STAT :, :].astype(F32)], axis=1
        )
        means.append(stat[0:1] + stat[1:2] + stat[2:3])
        seconds.append(stat[3:4] + stat[4:5] + stat[5:6])
        chan = p[rows + STAT :, :].astype(F32)
        gw.append(chan[6:7] + chan[7:8] + chan[8:9])
        b = chan[9:10] + chan[10:11] + chan[11:12]
        bw = b if bw is None else bw + b
        q = p[0:rows, :].astype(F32)
        total = q if total is None else total + q
    mean, rstd = combine_stats(means, seconds, width)
    table = jnp.concatenate(
        [m - mean for m in means] + [mean, rstd, jnp.zeros((126 - n, mean.shape[1]), F32)], axis=0
    )
    table = jnp.transpose(table)[0:rows]
    row_out[...] = table
    for k in range(n):
        total = total + table[:, k : k + 1] * gw[k]
    proj = (total * table[:, n + 1 : n + 2] + bw).astype(BF16)
    pooled_mix(sc, proj, group_map, gain, out, seq_length)


def normed(resid, table, gain, bias, n):
    return (resid - table[:, n : n + 1]) * table[:, n + 1 : n + 2] * gain + bias


def branch_resid(sc, mixed, own, oth, o_own, o_oth, scale):
    n = len(mixed)
    width = mixed[0].shape[1]
    acc_own, acc_oth = scale * own, scale * oth
    for k in range(n):
        rows = pl.ds(((sc[0] + n - k) % n) * width, width)
        block = mixed[k][...]
        acc_own = acc_own + dot(block, o_own[rows, :])
        acc_oth = acc_oth + dot(block, o_oth[rows, :])
    return acc_own, acc_oth


def centred(own, oth):
    width = own.shape[1] + oth.shape[1]
    mean = (jnp.sum(own, 1, keepdims=True) + jnp.sum(oth, 1, keepdims=True)) / width
    own, oth = own - mean, oth - mean
    second = jnp.sum(own * own, 1, keepdims=True) + jnp.sum(oth * oth, 1, keepdims=True)
    return own, oth, mean, second


def stat_rows(columns, rows, lanes):
    place = lax.broadcasted_iota(jnp.int32, (rows, 128), 1)
    table = jnp.zeros((rows, 128), F32)
    for i, c in enumerate(columns):
        table = jnp.where(place == i, c, table)
    if lanes > rows:
        table = jnp.concatenate([table, jnp.zeros((lanes - rows, 128), F32)], axis=0)
    return jnp.transpose(table)[0:STAT]


def streams_in(refs, first, rows, n):
    if first:
        own, oth, *rest = refs
        keep = slice(REACH, REACH + rows)
        return own[...].astype(F32)[keep], oth[...].astype(F32)[keep], rest
    own, oth, table, g_own, b_own, g_oth, b_oth, *rest = refs
    keep = slice(REACH, REACH + rows)
    t = table[keep, :]
    s_own = normed(own[keep, :], t, g_own[...], b_own[...], n).astype(BF16).astype(F32)
    s_oth = normed(oth[keep, :], t, g_oth[...], b_oth[...], n).astype(BF16).astype(F32)
    return s_own, s_oth, rest


def layer_body(sc, *refs, n, first, scale):
    mixed, refs = refs[:n], refs[n:]
    rows = mixed[0].shape[0]
    own, oth, refs = streams_in(refs, first, rows, n)
    o_own, o_oth, w_own, w_oth, g_own, b_own, g_oth, b_oth, *refs = refs
    outs, (r_own, r_oth, lhs_own, lhs_oth) = refs[:n], refs[n:]
    own, oth = branch_resid(sc, mixed, own, oth, o_own, o_oth, scale)
    r_own[...] = own
    r_oth[...] = oth
    own, oth, mean, second = centred(own, oth)
    width = outs[0].shape[1]
    stats = stat_rows(parts(mean) + parts(second), rows, 2 * width)
    for lhs, value, gain, bias in ((lhs_own, own, g_own, b_own), (lhs_oth, oth, g_oth, b_oth)):
        lhs[0:rows, :] = (value * gain[...]).astype(BF16)
        extra = parts(gain[...]) + parts(bias[...])
        extra = jnp.concatenate(
            list(extra) + [jnp.zeros((STAT - 6, value.shape[1]), F32)], axis=0
        )
        lhs[rows : rows + STAT, :] = extra.astype(BF16)
    place = lax.broadcasted_iota(jnp.int32, (STAT, width), 0)
    for k in range(n):
        at = pl.ds(((sc[0] + k) % n) * width, width)
        acc = dot_t(lhs_own[...], w_own[at, :]) + dot_t(lhs_oth[...], w_oth[at, :])
        outs[k][0:rows, :] = acc[0:rows].astype(BF16)
        tail = acc[rows : rows + STAT]
        sums = parts(tail[0:1] + tail[1:2] + tail[2:3]) + parts(tail[3:4] + tail[4:5] + tail[5:6])
        block = stats[:, width:]
        for i, s in enumerate(sums):
            block = jnp.where(place == 6 + i, s, block)
        outs[k][rows : rows + STAT, :] = stats[:, :width].astype(BF16)
        outs[k][rows + STAT :, :] = block.astype(BF16)


def last_body(sc, *refs, n, first, scale):
    mixed, refs = refs[:n], refs[n:]
    rows = mixed[0].shape[0]
    own, oth, refs = streams_in(refs, first, rows, n)
    o_own, o_oth, r_own, r_oth, stats = refs
    own, oth = branch_resid(sc, mixed, own, oth, o_own, o_oth, scale)
    r_own[...] = own
    r_oth[...] = oth
    _, _, mean, second = centred(own, oth)
    stats[...] = stat_rows((mean, second), rows, stats.shape[1])[0:8]


def finish_body(sc, *refs, n, width):
    stats, refs = refs[:n], refs[n:]
    r_own, r_oth, g_own, b_own, g_oth, b_oth, out_own, out_oth = refs
    rows = r_own.shape[0]
    mean, rstd = combine_stats([s[0:1, :] for s in stats], [s[1:2, :] for s in stats], width)
    table = jnp.concatenate([mean, rstd, jnp.zeros((126, mean.shape[1]), F32)], axis=0)
    table = jnp.transpose(table)[0:rows]
    out_own[...] = normed(r_own[...], table, g_own[...], b_own[...], 0).astype(BF16)
    out_oth[...] = normed(r_oth[...], table, g_oth[...], b_oth[...], 0).astype(BF16)


def place_body(sc, *refs):
    *blocks, out, sems = refs
    n = len(blocks)
    copies = []
    for k, block in enumerate(blocks):
        at = (sc[2] + n - k) % n
        copies.append(pltpu.make_async_copy(block, out.at[:, :, at], sems.at[k]))
    for c in copies:
        c.start()
    for c in copies:
        c.wait()


def shifted(array, axis, step):
    n = lax.axis_size(axis)
    return lax.ppermute(array, axis, [(i, (i + step) % n) for i in range(n)])


def gathered(shard, sc):
    nz, ny = lax.axis_size("z"), lax.axis_size("y")
    spread = jnp.broadcast_to(shard[None], (nz, *shard.shape))
    over_z = lax.all_to_all(spread, "z", 0, 0, tiled=True)
    over_y = [over_z] + [shifted(over_z, "y", k) for k in range(1, ny)]
    out = jax.ShapeDtypeStruct((nz, shard.shape[0], ny, *shard.shape[1:]), shard.dtype)
    anywhere = pl.BlockSpec(memory_space=pl.ANY)
    placed = kernel_call(
        place_body,
        out,
        scratch=[pltpu.SemaphoreType.DMA((ny,))],
        in_specs=[pl.BlockSpec(memory_space=pltpu.SMEM)] + [anywhere] * ny,
        out_specs=anywhere,
        name="place",
    )(sc, *over_y)
    return placed


def on_device(tokens, in_proj, group_mix, pool_gain, out_proj, norm_gain, norm_bias):
    rows_dev, feat = tokens.shape
    layers = in_proj.shape[0]
    n = lax.axis_size("x")
    sp = lax.axis_size(SP)
    seq_length = rows_dev * sp
    channels = in_proj.shape[2] * sp
    group = channels // n
    half_rows = rows_dev // 2
    pad = layers * REACH
    scale = (2.0 * layers) ** 0.25
    x, c = lax.axis_index("x"), lax.axis_index("c")
    start = lax.axis_index(SP) * rows_dev + c * half_rows

    def scalars(base):
        return jnp.stack([x, base, lax.axis_index("y"), c]).astype(jnp.int32)

    sc = scalars(start)
    in_t = jnp.swapaxes(in_proj, 1, 2)

    def other(array):
        return lax.ppermute(array, "c", [(0, 1), (1, 0)])

    def weights(*shards):
        placed = gathered(jnp.stack(shards), sc)
        both = (placed, other(placed))

        def pick(i):
            return [b[:, i].reshape(channels, feat) for b in both]

        return [pick(i) for i in range(len(shards))]

    (w_in,) = weights(in_t[0])

    up = [(i, i + 1) for i in range(sp - 1)]
    before = lax.ppermute(tokens[rows_dev - pad :], SP, up)
    after = lax.ppermute(tokens[:pad], SP, [(j, i) for i, j in up])
    wide = jnp.concatenate([before, tokens, after], axis=0)
    length = half_rows + 2 * pad
    mine = lax.dynamic_slice_in_dim(wide, c * half_rows, length, 0)
    theirs = other(lax.dynamic_slice_in_dim(wide, (1 - c) * half_rows, length, 0))
    norm = jnp.concatenate([norm_gain, norm_bias], axis=0)
    norms = (norm, other(norm))
    maps = lax.dynamic_index_in_dim(group_mix, x, 1, keepdims=False)
    gains = lax.dynamic_slice_in_dim(pool_gain, x * group, group, 1)

    def norm_rows(l):
        return [a[i : i + 1] for a in norms for i in (l, layers + l)]

    def block(rows, width, dtype=BF16):
        return jax.ShapeDtypeStruct((rows, width), dtype)

    def exchanged(blocks):
        return [blocks[0]] + [shifted(b, "x", k) for k, b in enumerate(blocks) if k]

    rows = length
    flops = 2 * rows * 2 * feat * channels
    partials = kernel_call(
        project_body, [block(rows, group)] * n, flops=flops, name="project"
    )(sc, mine, theirs, *w_in)
    stream = [mine, theirs]
    w_next = [weights(out_proj[l], in_t[l + 1]) for l in range(layers - 1)]
    w_next.append(weights(out_proj[layers - 1]))
    for l in range(layers):
        first, last = l == 0, l == layers - 1
        arrived = exchanged(partials)
        done = rows - 2 * REACH
        here = scalars(start - pad + (l + 1) * REACH)
        mix_flops = 2 * done * group * (rows + group)
        if first:
            mixed = kernel_call(
                functools.partial(mix_first_body, seq_length=seq_length),
                block(done, group),
                flops=mix_flops,
                name="mix",
            )(here, *arrived, maps[l], gains[l : l + 1])
        else:
            mixed, table = kernel_call(
                functools.partial(mix_body, seq_length=seq_length, width=2 * feat),
                [block(done, group), block(rows, 128, F32)],
                flops=mix_flops,
                name="mix",
            )(here, *arrived, maps[l], gains[l : l + 1])
            stream = stream + [table] + norm_rows(l - 1)
        all_mixed = exchanged([mixed] * n)
        rows = done
        resid = [block(rows, feat, F32)] * 2
        if not last:
            (o_own, o_oth), (w_own, w_oth) = w_next[l]
            *partials, r_own, r_oth = kernel_call(
                functools.partial(layer_body, n=n, first=first, scale=scale),
                [block(rows + 2 * STAT, group)] * n + resid,
                scratch=[pltpu.VMEM((rows + STAT, feat), BF16)] * 2,
                flops=4 * rows * 2 * feat * channels,
                name="layer",
            )(here, *all_mixed, *stream, o_own, o_oth, w_own, w_oth, *norm_rows(l))
            stream = [r_own, r_oth]
        else:
            ((o_own, o_oth),) = w_next[l]
            r_own, r_oth, stats = kernel_call(
                functools.partial(last_body, n=n, first=first, scale=scale),
                resid + [block(8, rows, F32)],
                flops=2 * rows * 2 * feat * channels,
                name="last",
            )(here, *all_mixed, *stream, o_own, o_oth)
            out_own, out_oth = kernel_call(
                functools.partial(finish_body, n=n, width=2 * feat),
                [block(rows, feat)] * 2,
                name="finish",
            )(here, *exchanged([stats] * n), r_own, r_oth, *norm_rows(l))
    swapped = other(out_oth)
    return jnp.where(
        c == 0,
        jnp.concatenate([out_own, swapped], axis=0),
        jnp.concatenate([swapped, out_own], axis=0),
    )


def solution(mesh):
    split = Mesh(mesh.devices.reshape(8, 4, 4, 2), ("z", "y", "x", "c"))
    tp = ("x", "c")
    in_specs = (P(SP, tp), P(None, tp, SP), P(), P(), P(None, SP, tp), P(None, tp), P(None, tp))
    return jax.shard_map(
        on_device, mesh=split, in_specs=in_specs, out_specs=P(SP, tp), check_vma=False
    )
```

time: 323 us -> 488 us (1.51)
  Pallas kernels: 0 us -> 231 us
  blocking collectives: 92.2 us -> 0 us
  starting transfers between devices: 43.4 us -> 101 us
  matrix products: 22.2 us -> 0 us
  local copies, waits for them, and re-layouts: 9.94 us -> 24.5 us
  between operations: 13.8 us -> 0.53 us
  waiting for transfers between devices: 133 us -> 122 us
    pallas_call x0 -> x12, Pallas kernels: none -> 231 us  [call(): pl.pallas_call(body, out_shape=out_shape, in_specs=specs, scratch_shapes=...]
    ppermute x6 -> x42, waiting for transfers between devices: 14.3 us -> 102 us  [the longest x33 101 us: shifted(): return lax.ppermute(array, axis, [(i, (i + step) % n) for i in range(n)])]
    all_to_all x5 -> x4, waiting for transfers between devices: 89.9 us -> 19.4 us  [gathered(): over_z = lax.all_to_all(spread, 'z', 0, 0, tiled=True)]
    all_to_all x4 -> x0, blocking collectives: 63.9 us -> none  [the longest x2 48 us: summed_on_arrival(): lax.all_to_all(blocks, axis, split_axis=0, concat_axis=0, tiled=True)]
    ppermute x6 -> x42, starting transfers between devices: 24.6 us -> 67.4 us  [the longest x33 57.5 us: shifted(): return lax.ppermute(array, axis, [(i, (i + step) % n) for i in range(n)])]
    all_gather x2 -> x0, waiting for transfers between devices: 29 us -> none  [gather_axes(): array = lax.all_gather(array, axis, axis=dim, tiled=True)]
    all_gather x2 -> x0, blocking collectives: 28.4 us -> none  [gather_axes(): array = lax.all_gather(array, axis, axis=dim, tiled=True)]
    dot_general x9 -> x0, matrix products: 22.2 us -> none  [the longest x3 9.99 us: on_device(): lax.dot_general(mixed_all, out_block, (((0,), (0,)), ((), ())), preferred...]
  transfers between devices with their start and end apart: 13 -> 46, of which waited for: 10 -> 23; matrix products, arithmetic and copies ran while one was open for 3% -> 4% of each run, Pallas kernels for 0% -> 46%
where the time goes in v1:
time: 488 us; the launch traced here: 483 us
  Pallas kernels  231 us (47%)
  waiting for transfers between devices  122 us (25%)
  starting transfers between devices  101 us (21%)
  local copies, waits for them, and re-layouts  24.5 us (5%)
    pallas_call x12, Pallas kernels, call(): pl.pallas_call(body, out_shape=out_shape, in_specs=specs, scratch_shapes=...  231 us
    ppermute x33, waiting for transfers between devices, shifted(): return lax.ppermute(array, axis, [(i, (i + step) % n) for i in range(n)])  101 us
    ppermute x33, starting transfers between devices, shifted(): return lax.ppermute(array, axis, [(i, (i + step) % n) for i in range(n)])  57.5 us
    all_to_all x4, starting transfers between devices, gathered(): over_z = lax.all_to_all(spread, 'z', 0, 0, tiled=True)  33.5 us
    all_to_all x4, waiting for transfers between devices, gathered(): over_z = lax.all_to_all(spread, 'z', 0, 0, tiled=True)  19.4 us
  transfers between devices with their start and end apart: 46, of which 23 were waited for; matrix products, arithmetic and copies ran while one was open for 4% of the time, Pallas kernels for 46%

profile of v1, /device:TPU:128, one launch (start us, length us, event | category | flops | bytes accessed | tf_op | source)
XLA Modules:
  0.0 482.5 jit_solution(7240399779611971259)
XLA Ops:
  1.6 7.2 %all-to-all-start = ((bf16[8,1,32,512]{3,2,1,0:T(8,128)(2,1)}), bf16[8,1,32,512]{3,2,1,0:T(8,128)(2,1)S(1)}, u32[]{:S(2)}, u32[]{:S(2)}) async-start(bf16[8,1,32,512]{3,2,1,0:T(8,128)(2,1)} %broadcast_in_dim.13), calls=%async_computation | async-start | bytes 524288 | tf_op jit(solution)/shard_map/all_to_all | solution.py:260
  8.8 6.5 %all-to-all-done.refs_0_ = bf16[8,1,32,512]{3,2,1,0:T(8,128)(2,1)S(1)} async-done(((bf16[8,1,32,512]{3,2,1,0:T(8,128)(2,1)}), bf16[8,1,32,512]{3,2,1,0:T(8,128)(2,1)S(1)}, u32[]{:S(2)}, u32[]{:S(2)}) %all-to-all-start) | async-done | bytes 262176 | tf_op jit(solution)/shard_map/all_to_all | solution.py:260
  16.2 8.8 %all-to-all-start.1 = ((bf16[8,2,32,512]{3,2,1,0:T(8,128)(2,1)}), bf16[8,2,32,512]{3,2,1,0:T(8,128)(2,1)S(1)}, u32[]{:S(2)}, u32[]{:S(2)}) async-start(bf16[8,2,32,512]{3,2,1,0:T(8,128)(2,1)} %broadcast_in_dim.28), calls=%async_computation.1 | async-start | bytes 1048576 | tf_op jit(solution)/shard_map/all_to_all | solution.py:260
  25.0 10.7 %all-to-all-done.1.refs_0_ = bf16[8,2,32,512]{3,2,1,0:T(8,128)(2,1)S(1)} async-done(((bf16[8,2,32,512]{3,2,1,0:T(8,128)(2,1)}), bf16[8,2,32,512]{3,2,1,0:T(8,128)(2,1)S(1)}, u32[]{:S(2)}, u32[]{:S(2)}) %all-to-all-start.1) | async-done | bytes 524320 | tf_op jit(solution)/shard_map/all_to_all | solution.py:260
  36.6 8.8 %all-to-all-start.2 = ((bf16[8,2,32,512]{3,2,1,0:T(8,128)(2,1)}), bf16[8,2,32,512]{3,2,1,0:T(8,128)(2,1)S(1)}, u32[]{:S(2)}, u32[]{:S(2)}) async-start(bf16[8,2,32,512]{3,2,1,0:T(8,128)(2,1)} %broadcast_in_dim.29), calls=%async_computation.2 | async-start | bytes 1048576 | tf_op jit(solution)/shard_map/all_to_all | solution.py:260
  56.2 8.7 %all-to-all-start.3 = ((bf16[8,1,32,512]{3,2,1,0:T(8,128)(2,1)}), bf16[8,1,32,512]{3,2,1,0:T(8,128)(2,1)S(1)}, u32[]{:S(2)}, u32[]{:S(2)}) async-start(bf16[8,1,32,512]{3,2,1,0:T(8,128)(2,1)} %broadcast_in_dim.31), calls=%async_computation.3 | async-start | bytes 524288 | tf_op jit(solution)/shard_map/all_to_all | solution.py:260
  64.9 6.4 %collective-permute-done.13.refs_1_ = bf16[8,2,32,512]{3,2,1,0:T(8,128)(2,1)S(1)} collective-permute-done((bf16[8,2,32,512]{3,2,1,0:T(8,128)(2,1)S(1)}, bf16[8,2,32,512]{3,2,1,0:T(8,128)(2,1)S(1)}, u32[]{:S(2)}, u32[]{:S(2)}) %collective-permute-start.13) | collective-permute-done | bytes 524320 | tf_op jit(solution)/shard_map/ppermute | solution.py:254
  74.1 65.3 %place.5 = bf16[8,2,4,32,512]{4,3,2,1,0:T(8,128)(2,1)} custom-call(s32[4]{0:T(128)} %add_add_fusion.sc, bf16[8,2,32,512]{3,2,1,0:T(8,128)(2,1)} %copy-done.4, bf16[8,2,32,512]{3,2,1,0:T(8,128)(2,1)} %copy-done.11, bf16[8,2,32,512]{3,2,1,0:T(8,128)(2,1)} %collective-permute-done.14.refs_2_, bf16[8,2,32,512]{3,2,1,0:T(8,128)(2,1)} %collective-permute-done.15.refs_3_), custom_call_target="tpu_custom_call" | custom-call | bytes 4194320 | tf_op jit(solution)/shard_map/place/pallas_call | solution.py:30
  140.1 3.5 collective-permute-start.25
  147.4 25.0 %collective-permute-done.5.refs_3_ = bf16[8,1,32,512]{3,2,1,0:T(8,128)(2,1)} collective-permute-done((bf16[8,1,32,512]{3,2,1,0:T(8,128)(2,1)S(1)}, bf16[8,1,32,512]{3,2,1,0:T(8,128)(2,1)}, u32[]{:S(2)}, u32[]{:S(2)}) %collective-permute-start.5) | collective-permute-done | bytes 262176 | tf_op jit(solution)/shard_map/ppermute | solution.py:254
  172.3 3.7 collective-permute-start
  176.0 33.6 %place.4 = bf16[8,1,4,32,512]{4,3,2,1,0:T(8,128)(2,1)} custom-call(s32[4]{0:T(128)} %add_add_fusion.sc, bf16[8,1,32,512]{3,2,1,0:T(8,128)(2,1)} %copy-done.6, bf16[8,1,32,512]{3,2,1,0:T(8,128)(2,1)} %collective-permute-done.3.refs_1_, bf16[8,1,32,512]{3,2,1,0:T(8,128)(2,1)} %collective-permute-done.4.refs_2_, ...), custom_call_target="tpu_custom_call" | custom-call | bytes 2097168 | tf_op jit(solution)/shard_map/place/pallas_call | solution.py:30
  211.2 5.5 %collective-permute-start.1 = (bf16[24,512]{1,0:T(8,128)(2,1)S(1)}, bf16[24,512]{1,0:T(8,128)(2,1)S(1)}, u32[]{:S(2)}, u32[]{:S(2)}) collective-permute-start(bf16[24,512]{1,0:T(8,128)(2,1)S(1)} %get-tuple-element.68), channel_id=1, source_target_pairs={{8,0},{16,8},{24,16},{32,24},{40,32},{48,40},{56,48},{64,56},{72,6... | collective-permute-start | bytes 73736 | tf_op jit(solution)/shard_map/ppermute | solution.py:311
  217.5 65.3 %place.6 = bf16[8,2,4,32,512]{4,3,2,1,0:T(8,128)(2,1)} custom-call(s32[4]{0:T(128)} %add_add_fusion.sc, bf16[8,2,32,512]{3,2,1,0:T(8,128)(2,1)} %copy-done.3, bf16[8,2,32,512]{3,2,1,0:T(8,128)(2,1)} %copy-done.8, bf16[8,2,32,512]{3,2,1,0:T(8,128)(2,1)} %copy-done.9, bf16[8,2,32,512]{3,2,1,0:T(8,128)(2,1)} %copy-done.10), custom_call_target="tpu_custom_call" | custom-call | bytes 4194320 | tf_op jit(solution)/shard_map/place/pallas_call | solution.py:30
  285.0 13.6 %collective-permute-done.34.refs_1_ = bf16[8,1,32,512]{3,2,1,0:T(8,128)(2,1)S(1)} collective-permute-done((bf16[8,1,32,512]{3,2,1,0:T(8,128)(2,1)S(1)}, bf16[8,1,32,512]{3,2,1,0:T(8,128)(2,1)S(1)}, u32[]{:S(2)}, u32[]{:S(2)}) %collective-permute-start.34) | collective-permute-done | bytes 262176 | tf_op jit(solution)/shard_map/ppermute | solution.py:254
  300.8 7.5 %collective-permute-done.36.refs_3_ = bf16[8,1,32,512]{3,2,1,0:T(8,128)(2,1)S(1)} collective-permute-done((bf16[8,1,32,512]{3,2,1,0:T(8,128)(2,1)S(1)}, bf16[8,1,32,512]{3,2,1,0:T(8,128)(2,1)S(1)}, u32[]{:S(2)}, u32[]{:S(2)}) %collective-permute-start.36) | collective-permute-done | bytes 262176 | tf_op jit(solution)/shard_map/ppermute | solution.py:254
  309.0 33.6 %place.7 = bf16[8,1,4,32,512]{4,3,2,1,0:T(8,128)(2,1)} custom-call(s32[4]{0:T(128)} %add_add_fusion.sc, bf16[8,1,32,512]{3,2,1,0:T(8,128)(2,1)} %copy-done.5, bf16[8,1,32,512]{3,2,1,0:T(8,128)(2,1)} %copy-done.12, bf16[8,1,32,512]{3,2,1,0:T(8,128)(2,1)} %copy-done.13, bf16[8,1,32,512]{3,2,1,0:T(8,128)(2,1)} %copy-done.14), custom_call_target="tpu_custom_call" | custom-call | bytes 2097168 | tf_op jit(solution)/shard_map/place/pallas_call | solution.py:30
  343.4 3.7 project.1
  355.9 5.5 %collective-permute-done.8.refs_2_ = bf16[432,256]{1,0:T(8,128)(2,1)} collective-permute-done((bf16[432,256]{1,0:T(8,128)(2,1)}, bf16[432,256]{1,0:T(8,128)(2,1)}, u32[]{:S(2)}, u32[]{:S(2)}) %collective-permute-start.8) | collective-permute-done | bytes 221216 | tf_op jit(solution)/shard_map/ppermute | solution.py:254
  369.3 3.1 fusion.2
  372.4 5.0 %collective-permute-done.11.refs_2_ = bf16[416,256]{1,0:T(8,128)(2,1)S(1)} collective-permute-done((bf16[416,256]{1,0:T(8,128)(2,1)}, bf16[416,256]{1,0:T(8,128)(2,1)S(1)}, u32[]{:S(2)}, u32[]{:S(2)}) %collective-permute-start.11) | collective-permute-done | bytes 213024 | tf_op jit(solution)/shard_map/ppermute | solution.py:254
  378.2 6.4 %layer.2 = (bf16[448,256]{1,0:T(8,128)(2,1)}, bf16[448,256]{1,0:T(8,128)(2,1)}, bf16[448,256]{1,0:T(8,128)(2,1)}, bf16[448,256]{1,0:T(8,128)(2,1)}, f32[416,512]{1,0:T(8,128)}, /*index=5*/f32[416,512]{1,0:T(8,128)}) custom-call(s32[4]{0:T(128)} %add_add_fusion.2.sc, bf16[416,256]{1,0:T(8,128)(2,1)} %mix.3.refs_0_, bf16[416,256]{1,0:T(8,128)(2,1)} %copy-done.32, ...), custom_call_target="tpu_custom_call" | custom-call | flops 1744830464 | bytes 8560656 | tf_op jit(solution)/shard_map/layer/pallas_call | solution.py:30
  390.2 3.3 collective-permute-done.18.refs_1_
  393.4 4.7 collective-permute-done.19.refs_2_
  401.2 10.7 %collective-permute-start.21 = (bf16[400,256]{1,0:T(8,128)(2,1)}, bf16[400,256]{1,0:T(8,128)(2,1)S(1)}, u32[]{:S(2)}, u32[]{:S(2)}) collective-permute-start(bf16[400,256]{1,0:T(8,128)(2,1)} %get-tuple-element.38.refs_0_), channel_id=1, source_target_pairs={{0,2},{2,4},{4,6},{6,0},{1,3},{3,5},{5,7},{7,1},{8,10},{10,12},{12... | collective-permute-start | bytes 614408 | tf_op jit(solution)/shard_map/ppermute | solution.py:254
  418.6 5.6 %collective-permute-done.22.refs_2_ = bf16[400,256]{1,0:T(8,128)(2,1)S(1)} collective-permute-done((bf16[400,256]{1,0:T(8,128)(2,1)}, bf16[400,256]{1,0:T(8,128)(2,1)S(1)}, u32[]{:S(2)}, u32[]{:S(2)}) %collective-permute-start.22) | collective-permute-done | bytes 204832 | tf_op jit(solution)/shard_map/ppermute | solution.py:254
  424.9 6.6 %layer.3 = (bf16[432,256]{1,0:T(8,128)(2,1)}, bf16[432,256]{1,0:T(8,128)(2,1)}, bf16[432,256]{1,0:T(8,128)(2,1)}, bf16[432,256]{1,0:T(8,128)(2,1)}, f32[400,512]{1,0:T(8,128)}, /*index=5*/f32[400,512]{1,0:T(8,128)}) custom-call(s32[4]{0:T(128)} %add_add_fusion.1.sc, bf16[400,256]{1,0:T(8,128)(2,1)} %get-tuple-element.38.refs_0_, ...), custom_call_target="tpu_custom_call" | custom-call | flops 1677721600 | bytes 9469968 | tf_op jit(solution)/shard_map/layer/pallas_call | solution.py:30
  435.8 3.8 collective-permute-done.28.refs_1_
  439.5 5.9 %collective-permute-done.29.refs_2_ = bf16[432,256]{1,0:T(8,128)(2,1)S(1)} collective-permute-done((bf16[432,256]{1,0:T(8,128)(2,1)}, bf16[432,256]{1,0:T(8,128)(2,1)S(1)}, u32[]{:S(2)}, u32[]{:S(2)}) %collective-permute-start.29) | collective-permute-done | bytes 221216 | tf_op jit(solution)/shard_map/ppermute | solution.py:254
  453.4 3.3 collective-permute-done.31.refs_1_
  456.7 5.4 %collective-permute-done.32.refs_2_ = bf16[384,256]{1,0:T(8,128)(2,1)S(1)} collective-permute-done((bf16[384,256]{1,0:T(8,128)(2,1)}, bf16[384,256]{1,0:T(8,128)(2,1)S(1)}, u32[]{:S(2)}, u32[]{:S(2)}) %collective-permute-start.32) | collective-permute-done | bytes 196640 | tf_op jit(solution)/shard_map/ppermute | solution.py:254
  462.8 4.5 last.1
  (167 shorter events, 90.8 us)
Async XLA Ops:
  1.6 13.7 %all-to-all-start = ((bf16[8,1,32,512]{3,2,1,0:T(8,128)(2,1)}), bf16[8,1,32,512]{3,2,1,0:T(8,128)(2,1)S(1)}, u32[]{:S(2)}, u32[]{:S(2)}) async-start(bf16[8,1,32,512]{3,2,1,0:T(8,128)(2,1)} %broadcast_in_dim.13), calls=%async_computation | async-start | bytes 524288 | tf_op jit(solution)/shard_map/all_to_all | solution.py:260
  16.2 19.5 %all-to-all-start.1 = ((bf16[8,2,32,512]{3,2,1,0:T(8,128)(2,1)}), bf16[8,2,32,512]{3,2,1,0:T(8,128)(2,1)S(1)}, u32[]{:S(2)}, u32[]{:S(2)}) async-start(bf16[8,2,32,512]{3,2,1,0:T(8,128)(2,1)} %broadcast_in_dim.28), calls=%async_computation.1 | async-start | bytes 1048576 | tf_op jit(solution)/shard_map/all_to_all | solution.py:260
  36.6 18.8 %all-to-all-start.2 = ((bf16[8,2,32,512]{3,2,1,0:T(8,128)(2,1)}), bf16[8,2,32,512]{3,2,1,0:T(8,128)(2,1)S(1)}, u32[]{:S(2)}, u32[]{:S(2)}) async-start(bf16[8,2,32,512]{3,2,1,0:T(8,128)(2,1)} %broadcast_in_dim.29), calls=%async_computation.2 | async-start | bytes 1048576 | tf_op jit(solution)/shard_map/all_to_all | solution.py:260
  45.4 25.9 %collective-permute-start.13 = (bf16[8,2,32,512]{3,2,1,0:T(8,128)(2,1)S(1)}, bf16[8,2,32,512]{3,2,1,0:T(8,128)(2,1)S(1)}, u32[]{:S(2)}, u32[]{:S(2)}) collective-permute-start(bf16[8,2,32,512]{3,2,1,0:T(8,128)(2,1)S(1)} %all-to-all-done.1.refs_0_), channel_id=1, source_target_pairs={{0,8},{8,16},{16,24},{24,0},{1,9},{9,17},{17,25},{25,1},{2,10},{10... | collective-permute-start | bytes 1572872 | tf_op jit(solution)/shard_map/ppermute | solution.py:254
  47.0 27.1 %collective-permute-start.14 = (bf16[8,2,32,512]{3,2,1,0:T(8,128)(2,1)S(1)}, bf16[8,2,32,512]{3,2,1,0:T(8,128)(2,1)}, u32[]{:S(2)}, u32[]{:S(2)}) collective-permute-start(bf16[8,2,32,512]{3,2,1,0:T(8,128)(2,1)S(1)} %all-to-all-done.1.refs_0_), channel_id=1, source_target_pairs={{0,16},{8,24},{16,0},{24,8},{1,17},{9,25},{17,1},{25,9},{2,18},{10... | collective-permute-start | bytes 1572872 | tf_op jit(solution)/shard_map/ppermute | solution.py:254
  49.9 24.2 %collective-permute-start.15 = (bf16[8,2,32,512]{3,2,1,0:T(8,128)(2,1)S(1)}, bf16[8,2,32,512]{3,2,1,0:T(8,128)(2,1)}, u32[]{:S(2)}, u32[]{:S(2)}) collective-permute-start(bf16[8,2,32,512]{3,2,1,0:T(8,128)(2,1)S(1)} %all-to-all-done.1.refs_0_), channel_id=1, source_target_pairs={{0,24},{8,0},{16,8},{24,16},{1,25},{9,1},{17,9},{25,17},{2,26},{10... | collective-permute-start | bytes 1572872 | tf_op jit(solution)/shard_map/ppermute | solution.py:254
  51.2 92.4 %collective-permute-start.3 = (bf16[8,1,32,512]{3,2,1,0:T(8,128)(2,1)S(1)}, bf16[8,1,32,512]{3,2,1,0:T(8,128)(2,1)}, u32[]{:S(2)}, u32[]{:S(2)}) collective-permute-start(bf16[8,1,32,512]{3,2,1,0:T(8,128)(2,1)S(1)} %all-to-all-done.refs_0_), channel_id=1, source_target_pairs={{0,8},{8,16},{16,24},{24,0},{1,9},{9,17},{17,25},{25,1},{2,10},{10... | collective-permute-start | bytes 786440 | tf_op jit(solution)/shard_map/ppermute | solution.py:254
  52.5 94.8 %collective-permute-start.4 = (bf16[8,1,32,512]{3,2,1,0:T(8,128)(2,1)S(1)}, bf16[8,1,32,512]{3,2,1,0:T(8,128)(2,1)}, u32[]{:S(2)}, u32[]{:S(2)}) collective-permute-start(bf16[8,1,32,512]{3,2,1,0:T(8,128)(2,1)S(1)} %all-to-all-done.refs_0_), channel_id=1, source_target_pairs={{0,16},{8,24},{16,0},{24,8},{1,17},{9,25},{17,1},{25,9},{2,18},{10... | collective-permute-start | bytes 786440 | tf_op jit(solution)/shard_map/ppermute | solution.py:254
  56.2 226.9 %all-to-all-start.3 = ((bf16[8,1,32,512]{3,2,1,0:T(8,128)(2,1)}), bf16[8,1,32,512]{3,2,1,0:T(8,128)(2,1)S(1)}, u32[]{:S(2)}, u32[]{:S(2)}) async-start(bf16[8,1,32,512]{3,2,1,0:T(8,128)(2,1)} %broadcast_in_dim.31), calls=%async_computation.3 | async-start | bytes 524288 | tf_op jit(solution)/shard_map/all_to_all | solution.py:260
  71.4 138.3 %collective-permute-start.24 = (bf16[8,2,32,512]{3,2,1,0:T(8,128)(2,1)S(1)}, bf16[8,2,32,512]{3,2,1,0:T(8,128)(2,1)S(1)}, u32[]{:S(2)}, u32[]{:S(2)}) collective-permute-start(bf16[8,2,32,512]{3,2,1,0:T(8,128)(2,1)S(1)} %all-to-all-done.2.refs_0_), channel_id=1, source_target_pairs={{0,8},{8,16},{16,24},{24,0},{1,9},{9,17},{17,25},{25,1},{2,10},{10... | collective-permute-start | bytes 1572872 | tf_op jit(solution)/shard_map/ppermute | solution.py:254
  139.4 228.3 %collective-permute-start.16 = (bf16[8,2,4,32,512]{4,3,2,1,0:T(8,128)(2,1)}, bf16[8,2,4,32,512]{4,3,2,1,0:T(8,128)(2,1)}, u32[]{:S(2)}, u32[]{:S(2)}) collective-permute-start(bf16[8,2,4,32,512]{4,3,2,1,0:T(8,128)(2,1)} %place.5), channel_id=1, source_target_pairs={{0,1},{1,0},{2,3},{3,2},{4,5},{5,4},{6,7},{7,6},{8,9},{9,8},{10,11... | collective-permute-start | bytes 6291464 | tf_op jit(solution)/shard_map/ppermute | solution.py:296
  140.1 71.1 %collective-permute-start.25 = (bf16[8,2,32,512]{3,2,1,0:T(8,128)(2,1)S(1)}, bf16[8,2,32,512]{3,2,1,0:T(8,128)(2,1)S(1)}, u32[]{:S(2)}, u32[]{:S(2)}) collective-permute-start(bf16[8,2,32,512]{3,2,1,0:T(8,128)(2,1)S(1)} %all-to-all-done.2.refs_0_), channel_id=1, source_target_pairs={{0,16},{8,24},{16,0},{24,8},{1,17},{9,25},{17,1},{25,9},{2,18},{10... | collective-permute-start | bytes 1572872 | tf_op jit(solution)/shard_map/ppermute | solution.py:254
  143.6 73.1 %collective-permute-start.26 = (bf16[8,2,32,512]{3,2,1,0:T(8,128)(2,1)S(1)}, bf16[8,2,32,512]{3,2,1,0:T(8,128)(2,1)S(1)}, u32[]{:S(2)}, u32[]{:S(2)}) collective-permute-start(bf16[8,2,32,512]{3,2,1,0:T(8,128)(2,1)S(1)} %all-to-all-done.2.refs_0_), channel_id=1, source_target_pairs={{0,24},{8,0},{16,8},{24,16},{1,25},{9,1},{17,9},{25,17},{2,26},{10... | collective-permute-start | bytes 1572872 | tf_op jit(solution)/shard_map/ppermute | solution.py:254
  147.3 25.1 %collective-permute-start.5 = (bf16[8,1,32,512]{3,2,1,0:T(8,128)(2,1)S(1)}, bf16[8,1,32,512]{3,2,1,0:T(8,128)(2,1)}, u32[]{:S(2)}, u32[]{:S(2)}) collective-permute-start(bf16[8,1,32,512]{3,2,1,0:T(8,128)(2,1)S(1)} %all-to-all-done.refs_0_), channel_id=1, source_target_pairs={{0,24},{8,0},{16,8},{24,16},{1,25},{9,1},{17,9},{25,17},{2,26},{10... | collective-permute-start | bytes 786440 | tf_op jit(solution)/shard_map/ppermute | solution.py:254
  172.3 110.5 %collective-permute-start = (bf16[24,512]{1,0:T(8,128)(2,1)S(1)}, bf16[24,512]{1,0:T(8,128)(2,1)S(1)}, u32[]{:S(2)}, u32[]{:S(2)}) collective-permute-start(bf16[24,512]{1,0:T(8,128)(2,1)S(1)} %get-tuple-element.69), channel_id=1, source_target_pairs={{0,8},{8,16},{16,24},{24,32},{32,40},{40,48},{48,56},{56,64},{64,7... | collective-permute-start | bytes 73736 | tf_op jit(solution)/shard_map/ppermute | solution.py:310
  209.6 133.0 %collective-permute-start.6 = (bf16[8,1,4,32,512]{4,3,2,1,0:T(8,128)(2,1)}, bf16[8,1,4,32,512]{4,3,2,1,0:T(8,128)(2,1)}, u32[]{:S(2)}, u32[]{:S(2)}) collective-permute-start(bf16[8,1,4,32,512]{4,3,2,1,0:T(8,128)(2,1)} %place.4), channel_id=1, source_target_pairs={{0,1},{1,0},{2,3},{3,2},{4,5},{5,4},{6,7},{7,6},{8,9},{9,8},{10,11... | collective-permute-start | bytes 3145736 | tf_op jit(solution)/shard_map/ppermute | solution.py:296
  211.2 72.1 %collective-permute-start.1 = (bf16[24,512]{1,0:T(8,128)(2,1)S(1)}, bf16[24,512]{1,0:T(8,128)(2,1)S(1)}, u32[]{:S(2)}, u32[]{:S(2)}) collective-permute-start(bf16[24,512]{1,0:T(8,128)(2,1)S(1)} %get-tuple-element.68), channel_id=1, source_target_pairs={{8,0},{16,8},{24,16},{32,24},{40,32},{48,40},{56,48},{64,56},{72,6... | collective-permute-start | bytes 73736 | tf_op jit(solution)/shard_map/ppermute | solution.py:311
  216.7 66.4 %collective-permute-start.17 = (f32[6,512]{1,0:T(8,128)S(1)}, f32[6,512]{1,0:T(8,128)S(1)}, u32[]{:S(2)}, u32[]{:S(2)}) collective-permute-start(f32[6,512]{1,0:T(8,128)S(1)} %pad_maximum_fusion.2), channel_id=1, source_target_pairs={{0,1},{1,0},{2,3},{3,2},{4,5},{5,4},{6,7},{7,6},{8,9},{9,8},{10,11... | collective-permute-start | bytes 36872 | tf_op jit(solution)/shard_map/ppermute | solution.py:296
  282.8 132.3 %collective-permute-start.27 = (bf16[8,2,4,32,512]{4,3,2,1,0:T(8,128)(2,1)}, bf16[8,2,4,32,512]{4,3,2,1,0:T(8,128)(2,1)}, u32[]{:S(2)}, u32[]{:S(2)}) collective-permute-start(bf16[8,2,4,32,512]{4,3,2,1,0:T(8,128)(2,1)} %place.6), channel_id=1, source_target_pairs={{0,1},{1,0},{2,3},{3,2},{4,5},{5,4},{6,7},{7,6},{8,9},{9,8},{10,11... | collective-permute-start | bytes 6291464 | tf_op jit(solution)/shard_map/ppermute | solution.py:296
  283.2 15.4 %collective-permute-start.34 = (bf16[8,1,32,512]{3,2,1,0:T(8,128)(2,1)S(1)}, bf16[8,1,32,512]{3,2,1,0:T(8,128)(2,1)S(1)}, u32[]{:S(2)}, u32[]{:S(2)}) collective-permute-start(bf16[8,1,32,512]{3,2,1,0:T(8,128)(2,1)S(1)} %all-to-all-done.3.refs_0_), channel_id=1, source_target_pairs={{0,8},{8,16},{16,24},{24,0},{1,9},{9,17},{17,25},{25,1},{2,10},{10... | collective-permute-start | bytes 786440 | tf_op jit(solution)/shard_map/ppermute | solution.py:254
  283.3 15.9 %collective-permute-start.35 = (bf16[8,1,32,512]{3,2,1,0:T(8,128)(2,1)S(1)}, bf16[8,1,32,512]{3,2,1,0:T(8,128)(2,1)S(1)}, u32[]{:S(2)}, u32[]{:S(2)}) collective-permute-start(bf16[8,1,32,512]{3,2,1,0:T(8,128)(2,1)S(1)} %all-to-all-done.3.refs_0_), channel_id=1, source_target_pairs={{0,16},{8,24},{16,0},{24,8},{1,17},{9,25},{17,1},{25,9},{2,18},{10... | collective-permute-start | bytes 786440 | tf_op jit(solution)/shard_map/ppermute | solution.py:254
  298.6 44.0 %collective-permute-start.2 = (bf16[432,512]{1,0:T(8,128)(2,1)S(1)}, bf16[432,512]{1,0:T(8,128)(2,1)S(1)}, u32[]{:S(2)}, u32[]{:S(2)}) collective-permute-start(bf16[432,512]{1,0:T(8,128)(2,1)S(1)} %get-tuple-element.66), channel_id=1, source_target_pairs={{0,1},{1,0},{2,3},{3,2},{4,5},{5,4},{6,7},{7,6},{8,9},{9,8},{10,11... | collective-permute-start | bytes 1327112 | tf_op jit(solution)/shard_map/ppermute | solution.py:296
  348.6 12.7 %collective-permute-start.8 = (bf16[432,256]{1,0:T(8,128)(2,1)}, bf16[432,256]{1,0:T(8,128)(2,1)}, u32[]{:S(2)}, u32[]{:S(2)}) collective-permute-start(bf16[432,256]{1,0:T(8,128)(2,1)} %get-tuple-element.32), channel_id=1, source_target_pairs={{0,4},{2,6},{4,0},{6,2},{1,5},{3,7},{5,1},{7,3},{8,12},{10,14},{12... | collective-permute-start | bytes 663560 | tf_op jit(solution)/shard_map/ppermute | solution.py:254
  355.8 97.5 %collective-permute-start.37 = (bf16[8,1,4,32,512]{4,3,2,1,0:T(8,128)(2,1)S(1)}, bf16[8,1,4,32,512]{4,3,2,1,0:T(8,128)(2,1)}, u32[]{:S(2)}, u32[]{:S(2)}) collective-permute-start(bf16[8,1,4,32,512]{4,3,2,1,0:T(8,128)(2,1)S(1)} %copy-done.2), channel_id=1, source_target_pairs={{0,1},{1,0},{2,3},{3,2},{4,5},{5,4},{6,7},{7,6},{8,9},{9,8},{10,11... | collective-permute-start | bytes 3145736 | tf_op jit(solution)/shard_map/ppermute | solution.py:296
  365.3 12.1 %collective-permute-start.11 = (bf16[416,256]{1,0:T(8,128)(2,1)}, bf16[416,256]{1,0:T(8,128)(2,1)S(1)}, u32[]{:S(2)}, u32[]{:S(2)}) collective-permute-start(bf16[416,256]{1,0:T(8,128)(2,1)} %mix.3.refs_0_), channel_id=1, source_target_pairs={{0,4},{2,6},{4,0},{6,2},{1,5},{3,7},{5,1},{7,3},{8,12},{10,14},{12... | collective-permute-start | bytes 638984 | tf_op jit(solution)/shard_map/ppermute | solution.py:254
  385.4 12.7 %collective-permute-start.19 = (bf16[448,256]{1,0:T(8,128)(2,1)}, bf16[448,256]{1,0:T(8,128)(2,1)}, u32[]{:S(2)}, u32[]{:S(2)}) collective-permute-start(bf16[448,256]{1,0:T(8,128)(2,1)} %get-tuple-element.36), channel_id=1, source_target_pairs={{0,4},{2,6},{4,0},{6,2},{1,5},{3,7},{5,1},{7,3},{8,12},{10,14},{12... | collective-permute-start | bytes 688136 | tf_op jit(solution)/shard_map/ppermute | solution.py:254
  388.1 10.1 %collective-permute-start.20 = (bf16[448,256]{1,0:T(8,128)(2,1)}, bf16[448,256]{1,0:T(8,128)(2,1)}, u32[]{:S(2)}, u32[]{:S(2)}) collective-permute-start(bf16[448,256]{1,0:T(8,128)(2,1)} %get-tuple-element.37), channel_id=1, source_target_pairs={{0,6},{2,0},{4,2},{6,4},{1,7},{3,1},{5,3},{7,5},{8,14},{10,8},{12,... | collective-permute-start | bytes 688136 | tf_op jit(solution)/shard_map/ppermute | solution.py:254
  401.2 17.4 %collective-permute-start.21 = (bf16[400,256]{1,0:T(8,128)(2,1)}, bf16[400,256]{1,0:T(8,128)(2,1)S(1)}, u32[]{:S(2)}, u32[]{:S(2)}) collective-permute-start(bf16[400,256]{1,0:T(8,128)(2,1)} %get-tuple-element.38.refs_0_), channel_id=1, source_target_pairs={{0,2},{2,4},{4,6},{6,0},{1,3},{3,5},{5,7},{7,1},{8,10},{10,12},{12... | collective-permute-start | bytes 614408 | tf_op jit(solution)/shard_map/ppermute | solution.py:254
  411.9 12.3 %collective-permute-start.22 = (bf16[400,256]{1,0:T(8,128)(2,1)}, bf16[400,256]{1,0:T(8,128)(2,1)S(1)}, u32[]{:S(2)}, u32[]{:S(2)}) collective-permute-start(bf16[400,256]{1,0:T(8,128)(2,1)} %get-tuple-element.38.refs_0_), channel_id=1, source_target_pairs={{0,4},{2,6},{4,0},{6,2},{1,5},{3,7},{5,1},{7,3},{8,12},{10,14},{12... | collective-permute-start | bytes 614408 | tf_op jit(solution)/shard_map/ppermute | solution.py:254
  432.5 13.0 %collective-permute-start.29 = (bf16[432,256]{1,0:T(8,128)(2,1)}, bf16[432,256]{1,0:T(8,128)(2,1)S(1)}, u32[]{:S(2)}, u32[]{:S(2)}) collective-permute-start(bf16[432,256]{1,0:T(8,128)(2,1)} %get-tuple-element.44), channel_id=1, source_target_pairs={{0,4},{2,6},{4,0},{6,2},{1,5},{3,7},{5,1},{7,3},{8,12},{10,14},{12... | collective-permute-start | bytes 663560 | tf_op jit(solution)/shard_map/ppermute | solution.py:254
  435.2 10.3 %collective-permute-start.30 = (bf16[432,256]{1,0:T(8,128)(2,1)}, bf16[432,256]{1,0:T(8,128)(2,1)S(1)}, u32[]{:S(2)}, u32[]{:S(2)}) collective-permute-start(bf16[432,256]{1,0:T(8,128)(2,1)} %get-tuple-element.45), channel_id=1, source_target_pairs={{0,6},{2,0},{4,2},{6,4},{1,7},{3,1},{5,3},{7,5},{8,14},{10,8},{12,... | collective-permute-start | bytes 663560 | tf_op jit(solution)/shard_map/ppermute | solution.py:254
  450.1 11.9 %collective-permute-start.32 = (bf16[384,256]{1,0:T(8,128)(2,1)}, bf16[384,256]{1,0:T(8,128)(2,1)S(1)}, u32[]{:S(2)}, u32[]{:S(2)}) collective-permute-start(bf16[384,256]{1,0:T(8,128)(2,1)} %get-tuple-element.46.refs_0_), channel_id=1, source_target_pairs={{0,4},{2,6},{4,0},{6,2},{1,5},{3,7},{5,1},{7,3},{8,12},{10,14},{12... | collective-permute-start | bytes 589832 | tf_op jit(solution)/shard_map/ppermute | solution.py:254
  (49 other events, 725.4 us)
